TPU v7x, 32 devices: a whole 2x2x4 slice. The times are simulated.
32 devices in a mesh: fs: 16 (over z, y, x), tp: 2 (over core).
Axes of the slice: x: 2, y: 2, z: 4, core: 2. Of those that a mesh axis runs over, the one named last changes fastest.
Arguments:
- tokens: bfloat16 [6144, 2048], P('fs', 'tp'), may hold values from -24 to 24, as said below
- mixer_gain: float32 [2048], replicated, may hold values from 0.1 to 1.9
- w_content: float32 [2048, 1024], P('fs', 'tp'), may hold values from -0.125 to 0.125
- w_spatial: float32 [2048, 1024], P('fs', 'tp'), may hold values from -0.125 to 0.125
- content_scale: float32 [1024], P('tp'), may hold values from 0.5 to 2
- spatial_scale: float32 [1024], P('tp'), may hold values from 0.2 to 3.5, as said below
- spatial_gain: float32 [1024], P('tp'), may hold values from 0.1 to 1.9
- block_mixing: bfloat16 [8, 128, 128], P('tp'), may hold values from -0.5 to 0.5
- block_bias: float32 [8, 128], P('tp'), may hold values from -6 to 6
- w_project: float32 [1024, 2048], P('tp', 'fs'), may hold values from -0.1875 to 0.1875
- project_scale: float32 [2048], P('fs'), may hold values from 0.5 to 2
- channel_gain: float32 [2048], replicated, may hold values from 0.1 to 1.9
- w_up: float32 [2048, 8192], P('fs', 'tp'), may hold values from -0.125 to 0.125
- up_scale: float32 [8192], P('tp'), may hold values from 0.5 to 2
- w_down: float32 [8192, 2048], P('tp', 'fs'), may hold values from -0.0625 to 0.0625
- down_scale: float32 [2048], P('fs'), may hold values from 0.5 to 2
Outputs:
- layer_out: bfloat16 [6144, 2048], P('fs', 'tp')
Inputs may be any that keep to these rules, and one draw needn't show every extreme that they name: `tokens`: activations whose features and rows have differing scales. `spatial_scale`: positive column scales.
All inputs are finite; a program needn't handle non-finite values.
Results may differ from a plain program's by a relative error of at most 0.019.
Values may be sent and summed in bfloat16 or wider, within the bound.
A program may use at most 128 MiB of HBM per device.

v0:
```python
import jax
import jax.numpy as jnp
from jax import lax
from jax.sharding import PartitionSpec as P

EPSILON = 1e-06


def normalize_rows(token_rows, gain_vector):
    values = token_rows.astype(jnp.float32)
    scaled = values * lax.rsqrt(jnp.mean(values * values, axis=-1, keepdims=True) + EPSILON)
    return (scaled * gain_vector).astype(jnp.bfloat16)


def shards(
    tokens,
    mixer_gain,
    w_content,
    w_spatial,
    content_scale,
    spatial_scale,
    spatial_gain,
    block_mixing,
    block_bias,
    w_project,
    project_scale,
    channel_gain,
    w_up,
    up_scale,
    w_down,
    down_scale,
):
    content_weight = w_content.astype(jnp.bfloat16)
    spatial_weight = w_spatial.astype(jnp.bfloat16)
    project_weight = w_project.astype(jnp.bfloat16)
    up_weight = w_up.astype(jnp.bfloat16)
    down_weight = w_down.astype(jnp.bfloat16)
    project_full, down_full = (
        lax.all_gather(project_scale, "fs", axis=0, tiled=True),
        lax.all_gather(down_scale, "fs", axis=0, tiled=True),
    )
    gathered_rows = lax.all_gather(tokens, "tp", axis=1, tiled=True)
    normed = normalize_rows(gathered_rows, mixer_gain)
    row_count = gathered_rows.shape[0]
    content_full, spatial_full, project_cols = (
        lax.all_gather(content_weight, "fs", axis=0, tiled=True),
        lax.all_gather(spatial_weight, "fs", axis=0, tiled=True),
        lax.all_gather(project_weight, "fs", axis=1, tiled=True),
    )
    content_linear = jnp.dot(normed, content_full, preferred_element_type=jnp.float32)
    spatial_linear = jnp.dot(normed, spatial_full, preferred_element_type=jnp.float32)
    content = jax.nn.gelu(content_linear * content_scale)
    spatial = jax.nn.gelu(spatial_linear * spatial_scale)
    square_sums = lax.psum(jnp.sum(spatial * spatial, axis=1), "tp")
    total_width = spatial.shape[1] * lax.axis_size("tp")
    spatial_norm = (
        spatial * lax.rsqrt(square_sums / total_width + EPSILON)[:, None] * spatial_gain
    ).astype(jnp.bfloat16)
    groups_here = block_mixing.shape[0]
    block_size = block_mixing.shape[1]
    group_width = spatial_norm.shape[1] // groups_here
    causal_mask = jnp.tril(jnp.ones((block_size, block_size), dtype=bool))
    mixing_weights = jnp.where(causal_mask[None, :, :], block_mixing, jnp.zeros_like(block_mixing))
    grouped = spatial_norm.reshape(row_count // block_size, block_size, groups_here, group_width)
    mixed_block = (
        jnp.einsum("gts,nsgc->ntgc", mixing_weights, grouped, preferred_element_type=jnp.float32)
        + block_bias.T[None, :, :, None]
    )
    gated = (content * mixed_block.reshape(row_count, spatial_norm.shape[1])).astype(jnp.bfloat16)
    mixer_terms = jnp.dot(gated, project_cols, preferred_element_type=jnp.float32) * project_full
    mixer_sum = lax.psum_scatter(
        mixer_terms.astype(jnp.bfloat16), "tp", scatter_dimension=1, tiled=True
    ).astype(jnp.float32)
    middle = (tokens.astype(jnp.float32) + mixer_sum).astype(jnp.bfloat16)
    middle_rows = lax.all_gather(middle, "tp", axis=1, tiled=True)
    channel_normed = normalize_rows(middle_rows, channel_gain)
    up_full, down_cols = (
        lax.all_gather(up_weight, "fs", axis=0, tiled=True),
        lax.all_gather(down_weight, "fs", axis=1, tiled=True),
    )
    up_linear = jnp.dot(channel_normed, up_full, preferred_element_type=jnp.float32)
    hidden = jnp.square(jax.nn.relu(up_linear * up_scale)).astype(jnp.bfloat16)
    channel_terms = jnp.dot(hidden, down_cols, preferred_element_type=jnp.float32) * down_full
    channel_sum = lax.psum_scatter(
        channel_terms.astype(jnp.bfloat16), "tp", scatter_dimension=1, tiled=True
    ).astype(jnp.float32)
    return (middle.astype(jnp.float32) + channel_sum).astype(jnp.bfloat16)


def solution(mesh):
    return jax.shard_map(
        shards,
        mesh=mesh,
        in_specs=(
            P("fs", "tp"),
            P(),
            P("fs", "tp"),
            P("fs", "tp"),
            P("tp"),
            P("tp"),
            P("tp"),
            P("tp", None, None),
            P("tp", None),
            P("tp", "fs"),
            P("fs"),
            P(),
            P("fs", "tp"),
            P("tp"),
            P("tp", "fs"),
            P("fs"),
        ),
        out_specs=P("fs", "tp"),
        check_vma=False,
    )
```

profile of v0, /device:TPU:1, one launch (start us, length us, event | category | flops | bytes accessed | tf_op | source)
XLA Modules:
  0.0 724.9 jit_solution(8672027433226947679)
XLA Ops:
  6.5 0.0 all-gather.10.cloned.1.call-start
  6.5 0.7 all-gather.10.cloned.1.call-update
  7.3 0.0 all-gather.14.cloned.1.call-start
  7.3 1.6 convert_element_type.64
  8.9 0.0 all-gather.14.cloned.1.call-update
  9.0 0.0 all-gather.12.cloned.1.call-start
  9.0 1.7 convert_element_type.63
  10.7 0.0 all-gather.12.cloned.1.call-update
  10.7 0.0 all-gather.16.cloned.1.call-start
  10.8 1.6 convert_element_type.67
  12.4 0.0 all-gather.16.cloned.1.call-update
  12.4 0.0 reduce-scatter.3.cloned.1.call-start
  12.4 0.0 copy-done.7
  12.5 34.5 %all-gather = f32[16,1,128]{2,1,0:T(1,128)S(1)} all-gather(f32[1,1,128]{2,1,0:T(1,128)S(1)} %bitcast.30), channel_id=1, replica_groups=mesh['fs'=16,'tp'=2] {'fs'}, dimensions={0}, use_global_device_ids=true | all-gather | bytes 8704 | tf_op jit(solution)/shard_map/all_gather | solution.py:39
  47.0 0.0 all-gather.10.cloned.1.call-done
  47.1 1.8 fusion.1
  48.9 0.0 copy-start.4
  48.9 0.0 copy-start.6
  48.9 35.3 %all-gather.14.cloned.1.call-done = bf16[2048,512]{1,0:T(8,128)(2,1)} async-done(((bf16[128,512]{1,0:T(8,128)(2,1)}), bf16[2048,512]{1,0:T(8,128)(2,1)}) %all-gather.14.cloned.1.call-update) | async-done | bytes 2097168 | tf_op jit(solution)/shard_map/all_gather | solution.py:47
  84.2 0.0 copy-done.10
  84.2 0.0 copy-done.12
  84.2 3.4 multiply_reduce_fusion
  87.6 3.7 psum.7
  91.3 0.0 copy-done.5
  91.3 0.1 multiply_convert_fusion.3
  91.5 0.0 copy-start.3
  91.5 0.0 copy-start.13
  91.5 0.1 reshape.39
  91.6 0.0 copy-done.4
  91.6 0.0 copy-done.6
  91.6 0.3 fusion.15
  92.0 0.3 copy.20
  92.3 53.9 %all-gather.12.cloned.1.call-done = bf16[2048,512]{1,0:T(8,128)(2,1)} async-done(((bf16[128,512]{1,0:T(8,128)(2,1)}), bf16[2048,512]{1,0:T(8,128)(2,1)}) %all-gather.12.cloned.1.call-update) | async-done | bytes 2097168 | tf_op jit(solution)/shard_map/all_gather | solution.py:46
  146.2 64.5 %all-gather.16.cloned.1.call-done = bf16[512,2048]{1,0:T(8,128)(2,1)} async-done(((bf16[512,128]{1,0:T(8,128)(2,1)}), bf16[512,2048]{1,0:T(8,128)(2,1)}) %all-gather.16.cloned.1.call-update) | async-done | bytes 2097168 | tf_op jit(solution)/shard_map/all_gather | solution.py:48
  210.7 0.0 copy-done.3
  210.7 0.0 copy-done.13
  210.7 5.5 multiply_convert_fusion.2
  216.2 0.0 reduce-scatter.3.cloned.1.call-update
  216.2 0.0 all-gather.18.cloned.1.call-start
  216.3 8.5 %reduce-scatter.3.cloned.1.call-done = bf16[384,1024]{1,0:T(8,128)(2,1)} async-done(((bf16[384,2048]{1,0:T(8,128)(2,1)}), bf16[384,1024]{1,0:T(8,128)(2,1)}) %reduce-scatter.3.cloned.1.call-update) | async-done | bytes 786448 | tf_op jit(solution)/shard_map/reduce_scatter | solution.py:71
  224.7 0.0 copy-done.1
  224.8 2.3 add_convert_fusion.1
  227.1 0.0 all-gather.18.cloned.1.call-update
  227.1 0.0 all-gather.20.cloned.1.call-start
  227.1 0.0 copy-done.2
  227.2 1.1 convert_element_type.74
  228.3 0.0 all-gather.20.cloned.1.call-update
  228.3 0.0 copy-start.8
  228.3 0.0 all-gather.22.cloned.1.call-start
  228.3 2.7 convert_element_type.76
  231.0 0.0 all-gather.22.cloned.1.call-update
  231.1 0.0 reduce-scatter.5.cloned.1.call-start
  231.1 0.0 copy-done.8
  231.1 34.2 %all-gather.1 = f32[16,1,128]{2,1,0:T(1,128)S(1)} all-gather(f32[1,1,128]{2,1,0:T(1,128)S(1)} %bitcast.31), channel_id=1, replica_groups=mesh['fs'=16,'tp'=2] {'fs'}, dimensions={0}, use_global_device_ids=true | all-gather | bytes 8704 | tf_op jit(solution)/shard_map/all_gather | solution.py:40
  265.3 1.8 fusion.4
  267.1 165.0 %all-gather.20.cloned.1.call-done = bf16[2048,4096]{1,0:T(8,128)(2,1)} async-done(((bf16[128,4096]{1,0:T(8,128)(2,1)}), bf16[2048,4096]{1,0:T(8,128)(2,1)}) %all-gather.20.cloned.1.call-update) | async-done | bytes 16777232 | tf_op jit(solution)/shard_map/all_gather | solution.py:78
  432.1 250.0 %all-gather.22.cloned.1.call-done = bf16[4096,2048]{1,0:T(8,128)(2,1)} async-done(((bf16[4096,128]{1,0:T(8,128)(2,1)}), bf16[4096,2048]{1,0:T(8,128)(2,1)}) %all-gather.22.cloned.1.call-update) | async-done | bytes 16777232 | tf_op jit(solution)/shard_map/all_gather | solution.py:79
  682.2 0.0 copy-done.9
  682.2 0.0 copy-done.11
  682.2 25.4 %multiply_convert_fusion.1 = bf16[384,2048]{1,0:T(8,128)(2,1)} fusion(bf16[4096,2048]{1,0:T(8,128)(2,1)} %all-gather.22.cloned.1.call-done, bf16[2048,4096]{1,0:T(8,128)(2,1)} %all-gather.20.cloned.1.call-done, f32[4096]{0:T(1024)S(1)} %copy-done.9, bf16[384,2048]{1,0:T(8,128)(2,1)} %all-gather.18.cloned.1.call-done, f32[2048]{0:T(1024)S(1)} %bitcast.28, ...), kind=kOutput, calls=%fused_computation.12 | convolution fusion | flops 12895911936 | bytes 36734464 | tf_op jit(solution)/shard_map/dot_general | solution.py:83
  707.6 0.0 reduce-scatter.5.cloned.1.call-update
  707.6 8.5 %reduce-scatter.5.cloned.1.call-done = bf16[384,1024]{1,0:T(8,128)(2,1)} async-done(((bf16[384,2048]{1,0:T(8,128)(2,1)}), bf16[384,1024]{1,0:T(8,128)(2,1)}) %reduce-scatter.5.cloned.1.call-update) | async-done | bytes 786448 | tf_op jit(solution)/shard_map/reduce_scatter | solution.py:84
  716.1 0.0 copy-done
  716.1 2.3 add_convert_fusion
  (14 shorter events, 0.1 us)
Async XLA Ops:
  6.5 5.9 copy-start.7
  6.5 77.7 %copy-start.10 = (f32[2048]{0:T(1024)S(1)}, f32[2048]{0:T(1024)}, u32[]{:S(2)}) copy-start(f32[2048]{0:T(1024)} %param.17) | copy-start | bytes 24580
  6.5 77.7 %copy-start.12 = (f32[512]{0:T(512)S(1)}, f32[512]{0:T(512)}, u32[]{:S(2)}) copy-start(f32[512]{0:T(512)} %param.21) | copy-start | bytes 6148
  6.5 40.5 %all-gather.10.cloned.1.call-start = ((), (), s32[]{:S(2)}) async-start(), calls=%async_computation.2 | async-start | bytes 2359296 | tf_op jit(solution)/shard_map/all_gather | solution.py:42
  7.3 76.9 %all-gather.14.cloned.1.call-start = ((), (), s32[]{:S(2)}) async-start(), calls=%async_computation.4 | async-start | bytes 2228224 | tf_op jit(solution)/shard_map/all_gather | solution.py:47
  9.0 137.2 %all-gather.12.cloned.1.call-start = ((), (), s32[]{:S(2)}) async-start(), calls=%async_computation.3 | async-start | bytes 2228224 | tf_op jit(solution)/shard_map/all_gather | solution.py:46
  10.7 200.0 %all-gather.16.cloned.1.call-start = ((), (), s32[]{:S(2)}) async-start(), calls=%async_computation.5 | async-start | bytes 2228224 | tf_op jit(solution)/shard_map/all_gather | solution.py:48
  12.4 212.3 %reduce-scatter.3.cloned.1.call-start = ((), (), s32[]{:S(2)}) async-start(), calls=%async_computation.6 | async-start | bytes 2359296 | tf_op jit(solution)/shard_map/reduce_scatter | solution.py:71
  48.9 42.5 %copy-start.5 = (f32[512]{0:T(512)S(1)}, f32[512]{0:T(512)}, u32[]{:S(2)}) copy-start(f32[512]{0:T(512)} %param.22) | copy-start | bytes 6148
  48.9 42.7 %copy-start.4 = (bf16[4,128,128]{2,1,0:T(8,128)(2,1)S(1)}, bf16[4,128,128]{2,1,0:T(8,128)(2,1)}, u32[]{:S(2)}) copy-start(bf16[4,128,128]{2,1,0:T(8,128)(2,1)} %param.23) | copy-start | bytes 393220
  48.9 42.7 %copy-start.6 = (f32[4,128]{1,0:T(4,128)S(1)}, f32[4,128]{1,0:T(4,128)}, u32[]{:S(2)}) copy-start(f32[4,128]{1,0:T(4,128)} %param.24) | copy-start | bytes 6148
  91.5 119.2 %copy-start.3 = (bf16[384,2048]{1,0:T(8,128)(2,1)S(1)}, bf16[384,2048]{1,0:T(8,128)(2,1)}, u32[]{:S(2)}) copy-start(bf16[384,2048]{1,0:T(8,128)(2,1)} %all-gather.10.cloned.1.call-done) | copy-start | bytes 4718596
  91.5 119.2 %copy-start.13 = (f32[512]{0:T(512)S(1)}, f32[512]{0:T(512)}, u32[]{:S(2)}) copy-start(f32[512]{0:T(512)} %param.20) | copy-start | bytes 6148
  216.2 8.6 %copy-start.1 = (bf16[384,1024]{1,0:T(8,128)(2,1)S(1)}, bf16[384,1024]{1,0:T(8,128)(2,1)}, u32[]{:S(2)}) copy-start(bf16[384,1024]{1,0:T(8,128)(2,1)} %param.16) | copy-start | bytes 2359300
  216.2 11.0 %copy-start.2 = (f32[128,4096]{1,0:T(8,128)S(1)}, f32[128,4096]{1,0:T(8,128)}, u32[]{:S(2)}) copy-start(f32[128,4096]{1,0:T(8,128)} %param.28) | copy-start | bytes 6291460
  216.2 49.1 %all-gather.18.cloned.1.call-start = ((), (), s32[]{:S(2)}) async-start(), calls=%async_computation.7 | async-start | bytes 2359296 | tf_op jit(solution)/shard_map/all_gather | solution.py:75
  227.1 205.0 %all-gather.20.cloned.1.call-start = ((), (), s32[]{:S(2)}) async-start(), calls=%async_computation.8 | async-start | bytes 17825792 | tf_op jit(solution)/shard_map/all_gather | solution.py:78
  228.3 2.8 copy-start.8
  228.3 453.9 %all-gather.22.cloned.1.call-start = ((), (), s32[]{:S(2)}) async-start(), calls=%async_computation.9 | async-start | bytes 17825792 | tf_op jit(solution)/shard_map/all_gather | solution.py:79
  231.0 451.1 %copy-start.9 = (f32[4096]{0:T(1024)S(1)}, f32[4096]{0:T(1024)}, u32[]{:S(2)}) copy-start(f32[4096]{0:T(1024)} %param.29) | copy-start | bytes 49156
  231.0 451.1 %copy-start.11 = (f32[2048]{0:T(1024)S(1)}, f32[2048]{0:T(1024)}, u32[]{:S(2)}) copy-start(f32[2048]{0:T(1024)} %param.27) | copy-start | bytes 24580
  231.1 485.0 %reduce-scatter.5.cloned.1.call-start = ((), (), s32[]{:S(2)}) async-start(), calls=%async_computation.10 | async-start | bytes 2359296 | tf_op jit(solution)/shard_map/reduce_scatter | solution.py:84
  707.6 8.5 %copy-start = (bf16[384,1024]{1,0:T(8,128)(2,1)S(1)}, bf16[384,1024]{1,0:T(8,128)(2,1)}, u32[]{:S(2)}) copy-start(bf16[384,1024]{1,0:T(8,128)(2,1)} %add_convert_fusion.1) | copy-start | bytes 2359300
Sparse Core Ops, SparseCore 0:
  8.9 12.2 all-gather.9
  23.9 60.2 all-gather.13
  87.0 59.1 all-gather.11
  148.7 61.8 all-gather.15
  216.3 8.3 reduce-scatter.2
  227.2 10.9 all-gather.17
  241.0 191.0 all-gather.19
  434.8 247.2 all-gather.21
  707.7 8.3 reduce-scatter.4
where the time goes:
time: 726 us; the launch traced here: 725 us
  waiting for transfers between devices  587 us (81%)
  blocking collectives  72.5 us (10%)
  matrix products  34.6 us (5%)
  other arithmetic  17.1 us (2%)
  between operations  13.4 us (2%)
    all_gather x1, waiting for transfers between devices, shards(): lax.all_gather(down_weight, 'fs', axis=1, tiled=True)  250 us
    all_gather x1, waiting for transfers between devices, shards(): lax.all_gather(up_weight, 'fs', axis=0, tiled=True)  165 us
    all_gather x1, waiting for transfers between devices, shards(): lax.all_gather(project_weight, 'fs', axis=1, tiled=True)  64.5 us
    all_gather x1, waiting for transfers between devices, shards(): lax.all_gather(content_weight, 'fs', axis=0, tiled=True)  53.9 us
    all_gather x1, waiting for transfers between devices, shards(): lax.all_gather(spatial_weight, 'fs', axis=0, tiled=True)  35.3 us
    all_gather x1, blocking collectives, shards(): lax.all_gather(project_scale, 'fs', axis=0, tiled=True)  34.5 us
    all_gather x1, blocking collectives, shards(): lax.all_gather(down_scale, 'fs', axis=0, tiled=True)  34.2 us
    dot_general x1, matrix products, shards(): jnp.dot(hidden, down_cols, preferred_element_type=jnp.float32) * down_full  25.4 us
  transfers between devices with their start and end apart: 9, of which 7 were waited for; matrix products, arithmetic and copies ran while one was open for 2% of the time, Pallas kernels for 0%

commit v1 on v0

--- a/solution.py
+++ b/solution.py
@@ -1,6 +1,10 @@
+import functools
+
 import jax
 import jax.numpy as jnp
 from jax import lax
+from jax.experimental import pallas as pl
+from jax.experimental.pallas import tpu as pltpu
 from jax.sharding import PartitionSpec as P
 
 EPSILON = 1e-06
@@ -87,9 +91,522 @@
     return (middle.astype(jnp.float32) + channel_sum).astype(jnp.bfloat16)
 
 
+PLANE = 4
+MESH = pl.DeviceIdType.MESH
+
+
+def layer_kernel(
+    sizes,
+    tokens_ref,
+    mixer_gain_ref,
+    content_ref,
+    spatial_ref,
+    content_scale_ref,
+    spatial_scale_ref,
+    spatial_gain_ref,
+    mixing_ref,
+    bias_ref,
+    project_ref,
+    project_scale_ref,
+    channel_gain_ref,
+    up_ref,
+    up_scale_ref,
+    down_ref,
+    down_scale_ref,
+    out_ref,
+    token_rows,
+    normed,
+    gate_weights,
+    project_full,
+    up_own,
+    down_own,
+    up_full,
+    down_full,
+    content_buf,
+    spatial_buf,
+    gated,
+    sums,
+    sums_in,
+    part,
+    part_in,
+    middle,
+    rows_all,
+    hidden,
+    terms,
+    terms_in,
+    results_in,
+    pair_send,
+    pair_recv,
+    swap_send,
+    swap_recv,
+    line_send,
+    line_recv,
+    gate_line_send,
+    gate_line_recv,
+    gate_send,
+    gate_recv,
+    row_send,
+    row_recv,
+    fwd_send,
+    fwd_recv,
+    term_send,
+    term_recv,
+    result_send,
+    result_recv,
+):
+    lines = sizes["lines"]
+    rows, half = tokens_ref.shape
+    width = token_rows.shape[1]
+    depth = content_ref.shape[0]
+    channels = content_ref.shape[1]
+    units = up_full.shape[1]
+    band = PLANE * depth
+    chunk = sizes["chunk"]
+    me = lax.axis_index("fs")
+    core = lax.axis_index("tp")
+    z = me // PLANE
+    p = me % PLANE
+    other = 1 - core
+    f32, bf16 = jnp.float32, jnp.bfloat16
+
+    def span(start, size, by=128):
+        return pl.ds(pl.multiple_of(start, by), size)
+
+    def peer(k):
+        return (p + k) % PLANE
+
+    def on_plane(k):
+        return {"fs": z * PLANE + peer(k)}
+
+    pair = {"tp": other}
+
+    def remote(src, dst, send, recv, where):
+        return pltpu.make_async_remote_copy(
+            src_ref=src, dst_ref=dst, send_sem=send, recv_sem=recv, device_id=where, device_id_type=MESH
+        )
+
+    barrier = pltpu.get_barrier_semaphore()
+    for k in range(1, PLANE):
+        pl.semaphore_signal(barrier, inc=1, device_id=on_plane(k), device_id_type=MESH)
+    pl.semaphore_signal(barrier, inc=1, device_id=pair, device_id_type=MESH)
+
+    @pl.when(z > 0)
+    def _():
+        pl.semaphore_signal(barrier, inc=1, device_id={"fs": me - PLANE}, device_id_type=MESH)
+
+    @pl.when(z < lines - 1)
+    def _():
+        pl.semaphore_signal(barrier, inc=1, device_id={"fs": me + PLANE}, device_id_type=MESH)
+
+    gate_weights[span(me * depth, depth), pl.ds(0, channels)] = content_ref[...].astype(bf16)
+    gate_weights[span(me * depth, depth), pl.ds(channels, channels)] = spatial_ref[...].astype(bf16)
+    project_full[:, span(me * depth, depth)] = (project_ref[...] * project_scale_ref[...]).astype(bf16)
+
+    @pl.loop(0, up_own.shape[1] // units)
+    def _(j):
+        up_own[:, span(j * units, units)] = up_ref[:, span(j * units, units)].astype(bf16)
+        down_own[span(j * units, units), :] = (
+            down_ref[span(j * units, units), :] * down_scale_ref[...]
+        ).astype(bf16)
+
+    up_full[span(me * depth, depth), :] = up_ref[:, span(p * units, units)].astype(bf16)
+    down_full[:, span(me * depth, depth)] = (
+        down_ref[span(p * units, units), :] * down_scale_ref[...]
+    ).astype(bf16)
+    token_rows[:, span(core * half, half)] = tokens_ref[...]
+
+    along = (z > 0).astype(jnp.int32) + (z < lines - 1).astype(jnp.int32)
+    pl.semaphore_wait(barrier, PLANE + along)
+
+    def gate_refs(owner):
+        return (
+            gate_weights.at[span(owner * depth, depth), :],
+            project_full.at[:, span(owner * depth, depth)],
+        )
+
+    def gate_line(block, side, step):
+        refs = gate_refs(block * PLANE + p)
+        return [
+            remote(
+                refs[a], refs[a], gate_line_send.at[a, side, block], gate_line_recv.at[a, block],
+                {"fs": me + step * PLANE},
+            )
+            for a in range(2)
+        ]
+
+    def gate_plane(block, k):
+        refs = gate_refs(block * PLANE + p)
+        return [
+            remote(refs[a], refs[a], gate_send.at[a, block, k], gate_recv.at[a, block, k], on_plane(k))
+            for a in range(2)
+        ]
+
+    def ff_line(a, block, side, step):
+        ref = up_full.at[span(block * band, band), :] if a == 0 else down_full.at[:, span(block * band, band)]
+        return remote(
+            ref, ref, line_send.at[a, side, block], line_recv.at[a, block], {"fs": me + step * PLANE}
+        )
+
+    def swap(a, k):
+        if a == 0:
+            src = up_own.at[:, span(peer(k) * units, units)]
+            dst = up_full.at[span(me * depth, depth), :]
+        else:
+            src = down_own.at[span(peer(k) * units, units), :]
+            dst = down_full.at[:, span(me * depth, depth)]
+        return remote(src, dst, swap_send.at[a, k], swap_recv.at[a, k], on_plane(k))
+
+    def swap_arrival(a, k):
+        owner = z * PLANE + (p + PLANE - k) % PLANE
+        dst = up_full.at[span(owner * depth, depth), :] if a == 0 else down_full.at[:, span(owner * depth, depth)]
+        return remote(dst, dst, swap_send.at[a, k], swap_recv.at[a, k], on_plane(k))
+
+    def both_sides(block, make):
+        @pl.when(z < lines - 1)
+        def _():
+            make(block, 0, 1)
+
+        @pl.when(z > 0)
+        def _():
+            make(block, 1, -1)
+
+    def start_gate(block, side, step):
+        for copy in gate_line(block, side, step):
+            copy.start()
+
+    token_copy = remote(
+        tokens_ref, token_rows.at[:, span(core * half, half)], pair_send.at[0], pair_recv.at[0], pair
+    )
+    token_copy.start()
+    both_sides(z, start_gate)
+    for a in range(2):
+        for k in range(1, PLANE):
+            swap(a, k).start()
+    for k in range(1, PLANE):
+        for copy in gate_plane(z, k):
+            copy.start()
+
+    token_copy.wait()
+
+    def normalize(source, gain_ref, target, first):
+        @pl.loop(0, rows // chunk)
+        def _(i):
+            values = source[span(i * chunk, chunk, chunk), :].astype(f32)
+            scaled = values * lax.rsqrt(jnp.mean(values * values, axis=-1, keepdims=True) + EPSILON)
+            target[span(first + i * chunk, chunk, chunk), :] = (scaled * gain_ref[...]).astype(bf16)
+
+    normalize(token_rows, mixer_gain_ref, normed, 0)
+
+    for d in range(1, lines):
+        for side, step in ((0, 1), (1, -1)):
+            block = z - step * d
+
+            @pl.when((block >= 0) & (block < lines))
+            def _(block=block, side=side, step=step):
+                for copy in gate_line(block, side, step):
+                    copy.wait_recv()
+
+                @pl.when((z + step >= 0) & (z + step < lines))
+                def _():
+                    start_gate(block, side, step)
+
+                for k in range(1, PLANE):
+                    for copy in gate_plane(block, k):
+                        copy.start()
+
+    for a in range(2):
+        for k in range(1, PLANE):
+            swap_arrival(a, k).wait_recv()
+        both_sides(z, lambda block, side, step, a=a: ff_line(a, block, side, step).start())
+
+    def relay(d, parts, forward):
+        for a in parts:
+            for side, step in ((0, 1), (1, -1)):
+                block = z - step * d
+
+                @pl.when((block >= 0) & (block < lines))
+                def _(a=a, block=block, side=side, step=step):
+                    ff_line(a, block, side, step).wait_recv()
+                    if forward:
+
+                        @pl.when((z + step >= 0) & (z + step < lines))
+                        def _():
+                            ff_line(a, block, side, step).start()
+
+    if lines > 2:
+        relay(1, (0, 1), True)
+
+    def gate_arrival(block, k):
+        refs = gate_refs(block * PLANE + (p + PLANE - k) % PLANE)
+        return [
+            remote(refs[a], refs[a], gate_send.at[a, block, k], gate_recv.at[a, block, k], on_plane(k))
+            for a in range(2)
+        ]
+
+    for block in range(lines):
+        for k in range(1, PLANE):
+            for copy in gate_arrival(block, k):
+                copy.wait_recv()
+
+    tile = sizes["tile"]
+
+    @pl.loop(0, channels // tile)
+    def _(j):
+        at = span(j * tile, tile)
+        linear = jnp.dot(normed[...], gate_weights[:, at], preferred_element_type=f32)
+        content_buf[:, at] = jax.nn.gelu(linear * content_scale_ref[:, at])
+        linear = jnp.dot(
+            normed[...], gate_weights[:, span(channels + j * tile, tile)], preferred_element_type=f32
+        )
+        spatial_buf[:, at] = jax.nn.gelu(linear * spatial_scale_ref[:, at])
+
+    spatial = spatial_buf[...]
+    sums[...] = jnp.broadcast_to(jnp.sum(spatial * spatial, axis=1, keepdims=True), sums.shape)
+    sum_copy = remote(sums, sums_in, pair_send.at[1], pair_recv.at[1], pair)
+    sum_copy.start()
+    sum_copy.wait()
+    groups, block_size = mixing_ref.shape[0], mixing_ref.shape[1]
+    group_width = channels // groups
+    causal = lax.broadcasted_iota(jnp.int32, (block_size, block_size), 0) >= lax.broadcasted_iota(
+        jnp.int32, (block_size, block_size), 1
+    )
+    for g in range(groups):
+        weights = jnp.where(causal, mixing_ref[g].astype(f32), 0.0).astype(bf16)
+        bias = jnp.broadcast_to(bias_ref[pl.ds(g, 1), :], (block_size, block_size)).T[:, :1]
+        at = pl.ds(g * group_width, group_width)
+        for n in range(rows // block_size):
+            these = pl.ds(n * block_size, block_size)
+            total = (sums[these, :1] + sums_in[these, :1]) / (2 * channels)
+            spatial_norm = (
+                spatial_buf[these, at] * lax.rsqrt(total + EPSILON) * spatial_gain_ref[:, at]
+            ).astype(bf16)
+            mixed = jnp.dot(weights, spatial_norm, preferred_element_type=f32) + bias
+            gated[these, at] = (content_buf[these, at] * mixed).astype(bf16)
+
+    @pl.loop(0, width // (2 * tile))
+    def _(j):
+        at = span(j * 2 * tile, 2 * tile)
+        part[:, at] = jnp.dot(gated[...], project_full[:, at], preferred_element_type=f32).astype(bf16)
+
+    part_copy = remote(part.at[:, span(other * half, half)], part_in, pair_send.at[2], pair_recv.at[2], pair)
+    part_copy.start()
+    part_copy.wait()
+    mine = span(core * half, half)
+
+    @pl.loop(0, rows // chunk)
+    def _(i):
+        these = span(i * chunk, chunk, chunk)
+        total = part[these, mine].astype(f32) + part_in[these, :].astype(f32)
+        middle[these, mine] = (tokens_ref[these, :].astype(f32) + total).astype(bf16)
+
+    middle_copy = remote(middle.at[:, mine], middle.at[:, mine], pair_send.at[3], pair_recv.at[3], pair)
+    middle_copy.start()
+    middle_copy.wait()
+    normalize(middle, channel_gain_ref, rows_all, p * rows)
+
+    own_rows = rows_all.at[span(p * rows, rows), mine]
+    row_copies = [remote(own_rows, own_rows, row_send.at[k], row_recv.at[k], on_plane(k)) for k in range(1, PLANE)]
+    for copy in row_copies:
+        copy.start()
+
+    for d in range(2, lines - 1):
+        relay(d, (0, 1), True)
+
+    forwards = []
+    for k in range(1, PLANE):
+        theirs = rows_all.at[span((p + PLANE - k) % PLANE * rows, rows), mine]
+        remote(theirs, theirs, row_send.at[k], row_recv.at[k], on_plane(k)).wait_recv()
+        forwards.append(remote(theirs, theirs, fwd_send.at[k], fwd_recv.at[k], pair))
+        forwards[-1].start()
+    for copy in forwards:
+        copy.wait_recv()
+
+    relay(lines - 1, (0,), False)
+
+    up_tile = sizes["up_tile"]
+
+    @pl.loop(0, PLANE)
+    def _(r):
+        these = span(r * rows, rows)
+
+        @pl.loop(0, units // up_tile)
+        def _(j):
+            at = span(j * up_tile, up_tile)
+            linear = jnp.dot(rows_all[these, :], up_full[:, at], preferred_element_type=f32)
+            linear = linear * up_scale_ref[:, span(p * units + j * up_tile, up_tile)]
+            hidden[these, at] = jnp.square(jnp.maximum(linear, 0.0)).astype(bf16)
+
+    per_core = lines // 2
+
+    def result_copy(block, k):
+        local = block % per_core
+        return remote(
+            terms.at[block, span(peer(k) * rows, rows), :],
+            results_in.at[k, local],
+            result_send.at[local, k],
+            result_recv.at[local, k],
+            on_plane(k),
+        )
+
+    def term_copy(block):
+        local = block % per_core
+        return remote(terms.at[block], terms_in.at[local], term_send.at[local], term_recv.at[local], pair)
+
+    for i in range(lines):
+        block = sizes["order"][0][i]
+        for row in range(1, lines):
+            block = jnp.where(z == row, sizes["order"][row][i], block)
+        if i == lines - 1:
+            relay(lines - 1, (1,), False)
+
+        @pl.loop(0, PLANE)
+        def _(r, block=block):
+            these = span(r * rows, rows)
+            terms[block, these, :] = jnp.dot(
+                hidden[these, :], down_full[:, span(block * band, band)], preferred_element_type=f32
+            ).astype(bf16)
+
+        @pl.when(block // per_core != core)
+        def _(block=block):
+            term_copy(block).start()
+
+        @pl.when(block // per_core == core)
+        def _(block=block):
+            term_copy(block).wait_recv()
+            local = block % per_core
+
+            @pl.loop(0, PLANE * rows // chunk)
+            def _(i):
+                these = span(i * chunk, chunk, chunk)
+                terms[block, these, :] = (
+                    terms[block, these, :].astype(f32) + terms_in[local, these, :].astype(f32)
+                ).astype(bf16)
+
+            for k in range(1, PLANE):
+                result_copy(block, k).start()
+
+    for i in range(per_core):
+        block = core * per_core + i
+        for k in range(1, PLANE):
+            result_copy(block, k).wait_recv()
+        at = pl.ds(i * band, band)
+
+        @pl.loop(0, rows // chunk)
+        def _(c, block=block, at=at, i=i):
+            these = span(c * chunk, chunk, chunk)
+            total = terms[block, span(p * rows + c * chunk, chunk, chunk), :].astype(f32)
+            for k in range(1, PLANE):
+                total = total + results_in[k, i, these, :].astype(f32)
+            out_ref[these, at] = (
+                middle[these, span(core * half + i * band, band)].astype(f32) + total
+            ).astype(bf16)
+
+    for k in range(1, PLANE):
+        for a in range(2):
+            swap(a, k).wait_send()
+        for block in range(lines):
+            for copy in gate_plane(block, k):
+                copy.wait_send()
+        row_copies[k - 1].wait_send()
+        forwards[k - 1].wait_send()
+        for i in range(per_core):
+            result_copy(core * per_core + i, k).wait_send()
+    for i in range(per_core):
+        term_copy(other * per_core + i).wait_send()
+    for side, step in ((0, 1), (1, -1)):
+        for d in range(lines):
+            block = z - step * d
+
+            @pl.when((block >= 0) & (block < lines) & (z + step >= 0) & (z + step < lines))
+            def _(block=block, side=side, step=step):
+                for copy in gate_line(block, side, step):
+                    copy.wait_send()
+                for a in range(2):
+                    ff_line(a, block, side, step).wait_send()
+
+
+def fused_shards(fs, tokens, mixer_gain, w_content, w_spatial, content_scale, spatial_scale, spatial_gain,
+                 block_mixing, block_bias, w_project, project_scale, channel_gain, w_up, up_scale, w_down, down_scale):
+    lines = fs // PLANE
+    rows, half = tokens.shape
+    width = 2 * half
+    channels = w_content.shape[1]
+    hidden_units = w_up.shape[1]
+    units = hidden_units // PLANE
+    depth = w_up.shape[0]
+    band = PLANE * depth
+    per_core = lines // 2
+    bf16, f32 = jnp.bfloat16, jnp.float32
+    order = [sorted(range(lines), key=lambda b, z=z: (abs(b - z), b)) for z in range(lines)]
+    sizes = dict(lines=lines, order=order, chunk=64, tile=256, up_tile=256)
+    vmem = pltpu.VMEM
+    dma = pltpu.SemaphoreType.DMA
+    row = lambda a: a.reshape(1, -1)
+    return pl.pallas_call(
+        functools.partial(layer_kernel, sizes),
+        out_shape=jax.ShapeDtypeStruct((rows, half), bf16),
+        in_specs=[pl.BlockSpec(memory_space=vmem)] * 16,
+        out_specs=pl.BlockSpec(memory_space=vmem),
+        scratch_shapes=[
+            vmem((rows, width), bf16),
+            vmem((rows, width), bf16),
+            vmem((width, 2 * channels), bf16),
+            vmem((channels, width), bf16),
+            vmem((depth, hidden_units), bf16),
+            vmem((hidden_units, depth), bf16),
+            vmem((width, units), bf16),
+            vmem((units, width), bf16),
+            vmem((rows, channels), f32),
+            vmem((rows, channels), f32),
+            vmem((rows, channels), bf16),
+            vmem((rows, 128), f32),
+            vmem((rows, 128), f32),
+            vmem((rows, width), bf16),
+            vmem((rows, half), bf16),
+            vmem((rows, width), bf16),
+            vmem((PLANE * rows, width), bf16),
+            vmem((PLANE * rows, units), bf16),
+            vmem((lines, PLANE * rows, band), bf16),
+            vmem((per_core, PLANE * rows, band), bf16),
+            vmem((PLANE, per_core, rows, band), bf16),
+            dma((4,)),
+            dma((4,)),
+            dma((2, PLANE)),
+            dma((2, PLANE)),
+            dma((2, 2, lines)),
+            dma((2, lines)),
+            dma((2, 2, lines)),
+            dma((2, lines)),
+            dma((2, lines, PLANE)),
+            dma((2, lines, PLANE)),
+            dma((PLANE,)),
+            dma((PLANE,)),
+            dma((PLANE,)),
+            dma((PLANE,)),
+            dma((per_core,)),
+            dma((per_core,)),
+            dma((per_core, PLANE)),
+            dma((per_core, PLANE)),
+        ],
+        compiler_params=pltpu.CompilerParams(
+            collective_id=0, has_side_effects=True, vmem_limit_bytes=VMEM_LIMIT
+        ),
+    )(tokens, row(mixer_gain), w_content, w_spatial, row(content_scale), row(spatial_scale), row(spatial_gain),
+      block_mixing, block_bias, w_project, row(project_scale), row(channel_gain), w_up, row(up_scale), w_down,
+      row(down_scale))
+
+
+VMEM_LIMIT = 67043328
+
+
 def solution(mesh):
+    fs, tp = mesh.shape["fs"], mesh.shape["tp"]
+    if tp == 2 and fs % (2 * PLANE) == 0 and fs <= 16:
+        body = functools.partial(fused_shards, fs)
+    else:
+        body = shards
     return jax.shard_map(
-        shards,
+        body,
         mesh=mesh,
         in_specs=(
             P("fs", "tp"),

time: 726 us -> 205 us (0.28)
  waiting for transfers between devices: 587 us -> 0 us
  Pallas kernels: 0 us -> 203 us
  blocking collectives: 72.5 us -> 0 us
  matrix products: 34.6 us -> 0 us
  other arithmetic: 17.1 us -> 0 us
  between operations: 13.4 us -> 0.01 us
    all_gather x7 -> x0, waiting for transfers between devices: 569 us -> none  [the longest x1 250 us: shards(): lax.all_gather(down_weight, 'fs', axis=1, tiled=True)]
    pallas_call x0 -> x1, Pallas kernels: none -> 203 us  [fused_shards(): pl.pallas_call(functools.partial(layer_kernel, sizes), out_shape=jax.Shap...]
    all_gather x2 -> x0, blocking collectives: 68.8 us -> none  [the longest x1 34.5 us: shards(): lax.all_gather(project_scale, 'fs', axis=0, tiled=True)]
    dot_general x4 -> x0, matrix products: 34.6 us -> none  [the longest x1 25.4 us: shards(): jnp.dot(hidden, down_cols, preferred_element_type=jnp.float32) * down_full]
    reduce_scatter x2 -> x0, waiting for transfers between devices: 17 us -> none  [the longest x1 8.5 us: shards(): lax.psum_scatter(mixer_terms.astype(jnp.bfloat16), 'tp', scatter_dimensio...]
    convert_element_type x8 -> x0, other arithmetic: 13.5 us -> none  [the longest x1 2.69 us: shards(): down_weight = w_down.astype(jnp.bfloat16)]
  transfers between devices with their start and end apart: 9 -> 0, of which waited for: 7 -> 0; matrix products, arithmetic and copies ran while one was open for 2% -> 0% of each run, Pallas kernels for 0% -> 0%
where the time goes in v1:
time: 205 us
  Pallas kernels  203 us (99%)
  local copies, waits for them, and re-layouts  2.06 us (1%)
    pallas_call x1, Pallas kernels, fused_shards(): pl.pallas_call(functools.partial(layer_kernel, sizes), out_shape=jax.Shap...  203 us

profile of v1, /device:TPU:1, one launch (start us, length us, event | category | flops | bytes accessed | tf_op | source)
XLA Modules:
  0.0 205.0 jit_solution(14699560770708837824)
XLA Ops:
  0.0 202.9 %shard_map.154 = bf16[384,1024]{1,0:T(8,128)(2,1)} custom-call(bf16[384,1024]{1,0:T(8,128)(2,1)} %tokens_ref.1, f32[1,2048]{1,0:T(1,128)} %bitcast.9, f32[128,512]{1,0:T(8,128)} %content_ref.1, f32[128,512]{1,0:T(8,128)} %spatial_ref.1, f32[1,512]{1,0:T(1,128)} %bitcast.11, f32[1,512]{1,0:T(1,128)} %bitcast.12, f32[1,512]{1,0:T(1,128)} %bitcast.13, ...), custom_call_target="tpu_custom_call" | custom-call | tf_op jit(solution)/shard_map/pallas_call | solution.py:545
  202.9 2.1 %copy.18 = bf16[384,1024]{1,0:T(8,128)(2,1)} copy(bf16[384,1024]{1,0:T(8,128)(2,1)} %shard_map.154) | data formatting | bytes 1572864

commit v2 on v1

--- a/solution.py
+++ b/solution.py
@@ -161,6 +161,7 @@
     channels = content_ref.shape[1]
     units = up_full.shape[1]
     band = PLANE * depth
+    piece = band // 2
     chunk = sizes["chunk"]
     me = lax.axis_index("fs")
     core = lax.axis_index("tp")
@@ -202,17 +203,6 @@
     gate_weights[span(me * depth, depth), pl.ds(channels, channels)] = spatial_ref[...].astype(bf16)
     project_full[:, span(me * depth, depth)] = (project_ref[...] * project_scale_ref[...]).astype(bf16)
 
-    @pl.loop(0, up_own.shape[1] // units)
-    def _(j):
-        up_own[:, span(j * units, units)] = up_ref[:, span(j * units, units)].astype(bf16)
-        down_own[span(j * units, units), :] = (
-            down_ref[span(j * units, units), :] * down_scale_ref[...]
-        ).astype(bf16)
-
-    up_full[span(me * depth, depth), :] = up_ref[:, span(p * units, units)].astype(bf16)
-    down_full[:, span(me * depth, depth)] = (
-        down_ref[span(p * units, units), :] * down_scale_ref[...]
-    ).astype(bf16)
     token_rows[:, span(core * half, half)] = tokens_ref[...]
 
     along = (z > 0).astype(jnp.int32) + (z < lines - 1).astype(jnp.int32)
@@ -242,7 +232,10 @@
         ]
 
     def ff_line(a, block, side, step):
-        ref = up_full.at[span(block * band, band), :] if a == 0 else down_full.at[:, span(block * band, band)]
+        if a == 0:
+            ref = up_full.at[span(block * band, band), :]
+        else:
+            ref = down_full.at[:, span(block * band + (a - 1) * piece, piece)]
         return remote(
             ref, ref, line_send.at[a, side, block], line_recv.at[a, block], {"fs": me + step * PLANE}
         )
@@ -279,6 +272,18 @@
     )
     token_copy.start()
     both_sides(z, start_gate)
+
+    @pl.loop(0, up_own.shape[1] // units)
+    def _(j):
+        up_own[:, span(j * units, units)] = up_ref[:, span(j * units, units)].astype(bf16)
+        down_own[span(j * units, units), :] = (
+            down_ref[span(j * units, units), :] * down_scale_ref[...]
+        ).astype(bf16)
+
+    up_full[span(me * depth, depth), :] = up_ref[:, span(p * units, units)].astype(bf16)
+    down_full[:, span(me * depth, depth)] = (
+        down_ref[span(p * units, units), :] * down_scale_ref[...]
+    ).astype(bf16)
     for a in range(2):
         for k in range(1, PLANE):
             swap(a, k).start()
@@ -317,7 +322,8 @@
     for a in range(2):
         for k in range(1, PLANE):
             swap_arrival(a, k).wait_recv()
-        both_sides(z, lambda block, side, step, a=a: ff_line(a, block, side, step).start())
+        for b in (0,) if a == 0 else (1, 2):
+            both_sides(z, lambda block, side, step, b=b: ff_line(b, block, side, step).start())
 
     def relay(d, parts, forward):
         for a in parts:
@@ -334,7 +340,7 @@
                             ff_line(a, block, side, step).start()
 
     if lines > 2:
-        relay(1, (0, 1), True)
+        relay(1, (0, 1, 2), True)
 
     def gate_arrival(block, k):
         refs = gate_refs(block * PLANE + (p + PLANE - k) % PLANE)
@@ -347,6 +353,9 @@
         for k in range(1, PLANE):
             for copy in gate_arrival(block, k):
                 copy.wait_recv()
+
+    for d in range(2, lines - 1):
+        relay(d, (0,), True)
 
     tile = sizes["tile"]
 
@@ -410,33 +419,35 @@
         copy.start()
 
     for d in range(2, lines - 1):
-        relay(d, (0, 1), True)
-
+        relay(d, (1, 2), True)
+    relay(lines - 1, (0,), False)
+
+    up_tile = sizes["up_tile"]
+
+    def raise_rows(owner):
+        these = span(owner * rows, rows)
+
+        @pl.loop(0, units // up_tile)
+        def _(j):
+            at = span(j * up_tile, up_tile)
+            linear = jnp.dot(rows_all[these, :], up_full[:, at], preferred_element_type=f32)
+            linear = linear * up_scale_ref[:, span(p * units + j * up_tile, up_tile)]
+            hidden[these, at] = jnp.square(jnp.maximum(linear, 0.0)).astype(bf16)
+
+    raise_rows(p)
     forwards = []
     for k in range(1, PLANE):
         theirs = rows_all.at[span((p + PLANE - k) % PLANE * rows, rows), mine]
         remote(theirs, theirs, row_send.at[k], row_recv.at[k], on_plane(k)).wait_recv()
         forwards.append(remote(theirs, theirs, fwd_send.at[k], fwd_recv.at[k], pair))
         forwards[-1].start()
-    for copy in forwards:
-        copy.wait_recv()
-
-    relay(lines - 1, (0,), False)
-
-    up_tile = sizes["up_tile"]
-
-    @pl.loop(0, PLANE)
-    def _(r):
-        these = span(r * rows, rows)
-
-        @pl.loop(0, units // up_tile)
-        def _(j):
-            at = span(j * up_tile, up_tile)
-            linear = jnp.dot(rows_all[these, :], up_full[:, at], preferred_element_type=f32)
-            linear = linear * up_scale_ref[:, span(p * units + j * up_tile, up_tile)]
-            hidden[these, at] = jnp.square(jnp.maximum(linear, 0.0)).astype(bf16)
-
-    per_core = lines // 2
+        if k > 1:
+            forwards[k - 2].wait_recv()
+            raise_rows((p + PLANE - k + 1) % PLANE)
+    forwards[-1].wait_recv()
+    raise_rows((p + 1) % PLANE)
+
+    per_core = lines
 
     def result_copy(block, k):
         local = block % per_core
@@ -452,18 +463,19 @@
         local = block % per_core
         return remote(terms.at[block], terms_in.at[local], term_send.at[local], term_recv.at[local], pair)
 
-    for i in range(lines):
-        block = sizes["order"][0][i]
+    for i in range(2 * lines):
+        block = sizes["order"][0][i // 2]
         for row in range(1, lines):
-            block = jnp.where(z == row, sizes["order"][row][i], block)
-        if i == lines - 1:
-            relay(lines - 1, (1,), False)
+            block = jnp.where(z == row, sizes["order"][row][i // 2], block)
+        block = 2 * block + i % 2
+        if i >= 2 * lines - 2:
+            relay(lines - 1, (1 + i % 2,), False)
 
         @pl.loop(0, PLANE)
         def _(r, block=block):
             these = span(r * rows, rows)
             terms[block, these, :] = jnp.dot(
-                hidden[these, :], down_full[:, span(block * band, band)], preferred_element_type=f32
+                hidden[these, :], down_full[:, span(block * piece, piece)], preferred_element_type=f32
             ).astype(bf16)
 
         @pl.when(block // per_core != core)
@@ -489,7 +501,7 @@
         block = core * per_core + i
         for k in range(1, PLANE):
             result_copy(block, k).wait_recv()
-        at = pl.ds(i * band, band)
+        at = pl.ds(i * piece, piece)
 
         @pl.loop(0, rows // chunk)
         def _(c, block=block, at=at, i=i):
@@ -498,7 +510,7 @@
             for k in range(1, PLANE):
                 total = total + results_in[k, i, these, :].astype(f32)
             out_ref[these, at] = (
-                middle[these, span(core * half + i * band, band)].astype(f32) + total
+                middle[these, span(core * half + i * piece, piece)].astype(f32) + total
             ).astype(bf16)
 
     for k in range(1, PLANE):
@@ -521,7 +533,7 @@
             def _(block=block, side=side, step=step):
                 for copy in gate_line(block, side, step):
                     copy.wait_send()
-                for a in range(2):
+                for a in range(3):
                     ff_line(a, block, side, step).wait_send()
 
 
@@ -535,7 +547,8 @@
     units = hidden_units // PLANE
     depth = w_up.shape[0]
     band = PLANE * depth
-    per_core = lines // 2
+    per_core = lines
+    piece = band // 2
     bf16, f32 = jnp.bfloat16, jnp.float32
     order = [sorted(range(lines), key=lambda b, z=z: (abs(b - z), b)) for z in range(lines)]
     sizes = dict(lines=lines, order=order, chunk=64, tile=256, up_tile=256)
@@ -566,15 +579,15 @@
             vmem((rows, width), bf16),
             vmem((PLANE * rows, width), bf16),
             vmem((PLANE * rows, units), bf16),
-            vmem((lines, PLANE * rows, band), bf16),
-            vmem((per_core, PLANE * rows, band), bf16),
-            vmem((PLANE, per_core, rows, band), bf16),
+            vmem((2 * lines, PLANE * rows, piece), bf16),
+            vmem((per_core, PLANE * rows, piece), bf16),
+            vmem((PLANE, per_core, rows, piece), bf16),
             dma((4,)),
             dma((4,)),
             dma((2, PLANE)),
             dma((2, PLANE)),
-            dma((2, 2, lines)),
-            dma((2, lines)),
+            dma((3, 2, lines)),
+            dma((3, lines)),
             dma((2, 2, lines)),
             dma((2, lines)),
             dma((2, lines, PLANE)),

time: 205 us -> 209 us (1.020)
  Pallas kernels: 203 us -> 206 us
    pallas_call x1, Pallas kernels: 203 us -> 206 us  [fused_shards(): pl.pallas_call(functools.partial(layer_kernel, sizes), out_shape=jax.Shap...]
where the time goes in v2:
time: 209 us; the launch traced here: 208 us
  Pallas kernels  206 us (99%)
    pallas_call x1, Pallas kernels, fused_shards(): pl.pallas_call(functools.partial(layer_kernel, sizes), out_shape=jax.Shap...  206 us

profile of v2, /device:TPU:1, one launch (start us, length us, event | category | flops | bytes accessed | tf_op | source)
XLA Modules:
  0.0 208.4 jit_solution(10383690636399512523)
XLA Ops:
  0.0 206.3 %shard_map.154 = bf16[384,1024]{1,0:T(8,128)(2,1)} custom-call(bf16[384,1024]{1,0:T(8,128)(2,1)} %tokens_ref.1, f32[1,2048]{1,0:T(1,128)} %bitcast.9, f32[128,512]{1,0:T(8,128)} %content_ref.1, f32[128,512]{1,0:T(8,128)} %spatial_ref.1, f32[1,512]{1,0:T(1,128)} %bitcast.11, f32[1,512]{1,0:T(1,128)} %bitcast.12, f32[1,512]{1,0:T(1,128)} %bitcast.13, ...), custom_call_target="tpu_custom_call" | custom-call | tf_op jit(solution)/shard_map/pallas_call | solution.py:558
  206.3 2.1 copy.18

commit v3 on v1

--- a/solution.py
+++ b/solution.py
@@ -109,11 +109,14 @@
     project_ref,
     project_scale_ref,
     channel_gain_ref,
-    up_ref,
+    up_hbm,
     up_scale_ref,
-    down_ref,
+    down_hbm,
     down_scale_ref,
     out_ref,
+    up_ref,
+    down_ref,
+    load_sem,
     token_rows,
     normed,
     gate_weights,
@@ -185,6 +188,12 @@
             src_ref=src, dst_ref=dst, send_sem=send, recv_sem=recv, device_id=where, device_id_type=MESH
         )
 
+    loads = [
+        pltpu.make_async_copy(up_hbm, up_ref, load_sem.at[0]),
+        pltpu.make_async_copy(down_hbm, down_ref, load_sem.at[1]),
+    ]
+    for load in loads:
+        load.start()
     barrier = pltpu.get_barrier_semaphore()
     for k in range(1, PLANE):
         pl.semaphore_signal(barrier, inc=1, device_id=on_plane(k), device_id_type=MESH)
@@ -202,17 +211,6 @@
     gate_weights[span(me * depth, depth), pl.ds(channels, channels)] = spatial_ref[...].astype(bf16)
     project_full[:, span(me * depth, depth)] = (project_ref[...] * project_scale_ref[...]).astype(bf16)
 
-    @pl.loop(0, up_own.shape[1] // units)
-    def _(j):
-        up_own[:, span(j * units, units)] = up_ref[:, span(j * units, units)].astype(bf16)
-        down_own[span(j * units, units), :] = (
-            down_ref[span(j * units, units), :] * down_scale_ref[...]
-        ).astype(bf16)
-
-    up_full[span(me * depth, depth), :] = up_ref[:, span(p * units, units)].astype(bf16)
-    down_full[:, span(me * depth, depth)] = (
-        down_ref[span(p * units, units), :] * down_scale_ref[...]
-    ).astype(bf16)
     token_rows[:, span(core * half, half)] = tokens_ref[...]
 
     along = (z > 0).astype(jnp.int32) + (z < lines - 1).astype(jnp.int32)
@@ -279,6 +277,20 @@
     )
     token_copy.start()
     both_sides(z, start_gate)
+    for load in loads:
+        load.wait()
+
+    @pl.loop(0, up_own.shape[1] // units)
+    def _(j):
+        up_own[:, span(j * units, units)] = up_ref[:, span(j * units, units)].astype(bf16)
+        down_own[span(j * units, units), :] = (
+            down_ref[span(j * units, units), :] * down_scale_ref[...]
+        ).astype(bf16)
+
+    up_full[span(me * depth, depth), :] = up_ref[:, span(p * units, units)].astype(bf16)
+    down_full[:, span(me * depth, depth)] = (
+        down_ref[span(p * units, units), :] * down_scale_ref[...]
+    ).astype(bf16)
     for a in range(2):
         for k in range(1, PLANE):
             swap(a, k).start()
@@ -545,9 +557,14 @@
     return pl.pallas_call(
         functools.partial(layer_kernel, sizes),
         out_shape=jax.ShapeDtypeStruct((rows, half), bf16),
-        in_specs=[pl.BlockSpec(memory_space=vmem)] * 16,
+        in_specs=[
+            pl.BlockSpec(memory_space=pl.ANY if i in (12, 14) else vmem) for i in range(16)
+        ],
         out_specs=pl.BlockSpec(memory_space=vmem),
         scratch_shapes=[
+            vmem((depth, hidden_units), f32),
+            vmem((hidden_units, depth), f32),
+            dma((2,)),
             vmem((rows, width), bf16),
             vmem((rows, width), bf16),
             vmem((width, 2 * channels), bf16),

time: 205 us -> 204 us (level)
  no operation moved by 1% of the time
where the time goes in v3:
time: 204 us
  Pallas kernels  202 us (99%)
  local copies, waits for them, and re-layouts  2.06 us (1%)
    pallas_call x1, Pallas kernels, fused_shards(): pl.pallas_call(functools.partial(layer_kernel, sizes), out_shape=jax.Shap...  202 us

profile of v3, /device:TPU:1, one launch (start us, length us, event | category | flops | bytes accessed | tf_op | source)
XLA Modules:
  0.0 204.1 jit_solution(3821672602934845529)
XLA Ops:
  0.0 202.0 %shard_map.154 = bf16[384,1024]{1,0:T(8,128)(2,1)} custom-call(bf16[384,1024]{1,0:T(8,128)(2,1)} %tokens_ref.1, f32[1,2048]{1,0:T(1,128)} %bitcast.9, f32[128,512]{1,0:T(8,128)} %content_ref.1, f32[128,512]{1,0:T(8,128)} %spatial_ref.1, f32[1,512]{1,0:T(1,128)} %bitcast.11, f32[1,512]{1,0:T(1,128)} %bitcast.12, f32[1,512]{1,0:T(1,128)} %bitcast.13, ...), custom_call_target="tpu_custom_call" | custom-call | tf_op jit(solution)/shard_map/pallas_call | solution.py:557
  202.0 2.1 %copy.18 = bf16[384,1024]{1,0:T(8,128)(2,1)} copy(bf16[384,1024]{1,0:T(8,128)(2,1)} %shard_map.154) | data formatting | bytes 1572864
